TPU v7x, 32 devices: a whole 2x2x4 slice. The times are simulated.
32 devices in a mesh: grp: 2 (over y), sp: 4 (over z), tp: 4 (over x, core).
Axes of the slice: x: 2, y: 2, z: 4, core: 2. Of those that a mesh axis runs over, the one named last changes fastest.
Arguments:
- stream: bfloat16 [12288, 4096], P(('grp', 'sp', 'tp')), parts along dimension 0, may hold values from -6 to 6
- norm_gain: float32 [2, 4096], replicated, may hold values from 0.1 to 1.9
- mix_weight: bfloat16 [2, 4, 1024, 1024], P(None, None, 'sp', 'tp'), may hold values from -0.1875 to 0.1875
- branch_scale: float32 [2, 4096], replicated, may hold values from 0.1 to 1.9
Outputs:
- result: bfloat16 [12288, 4096], P(('grp', 'sp', 'tp')), parts along dimension 0
There are 2 independent parts, one for each index of `grp`. A program takes and returns all parts, laid end to end along the dimension named above; an argument that names none is the same for every part. Nothing has to cross between parts.
All inputs are finite; a program needn't handle non-finite values.
Results may differ from a plain program's by a relative error of at most 0.0056.
Values may be sent and summed in bfloat16 or wider, within the bound.
A program may use at most 128 MiB of HBM per device.

v0:
```python
import jax
import jax.numpy as jnp
from jax import lax
from jax.sharding import PartitionSpec as P

GW = 1024
G = 4
LAYERS = 2
epsilon = 1e-06
window_lengths = (2, 4, 8, 16)
halo_rows = 15


def from_behind(block, axis, distance):
    devices = range(lax.axis_size(axis))
    route = [(i - distance, i) for i in devices if i - distance in devices]
    return lax.ppermute(block, axis, route)


def per_device(stream, norm_gain, mix_weight, branch_scale):
    row_count = stream.shape[0]
    feature_width = stream.shape[1]
    offset = lax.axis_index(("sp", "tp")) * row_count
    counts_base = (offset + lax.iota(jnp.int32, row_count)).astype(jnp.float32) + 1.0
    residual = stream.astype(jnp.float32)
    for layer_idx in range(LAYERS):
        scale_rows = lax.rsqrt(jnp.mean(residual * residual, axis=1, keepdims=True) + epsilon)
        normed = (residual * scale_rows * norm_gain[layer_idx]).astype(jnp.bfloat16)
        earlier = from_behind(normed[row_count - halo_rows :], ("sp", "tp"), 1)
        extended = jnp.concatenate([earlier, normed], axis=0).astype(jnp.float32)
        pieces = []
        for group_idx in range(G):
            window_len = window_lengths[group_idx]
            segment = extended[:, group_idx * GW : (group_idx + 1) * GW]
            own_rows = segment[halo_rows:]
            running = own_rows
            for back_step in range(1, window_len):
                running = (
                    running + segment[halo_rows - back_step : halo_rows - back_step + row_count]
                )
            window_mean = running / jnp.minimum(counts_base, float(window_len))[:, None]
            pieces.append((window_mean - own_rows).astype(jnp.bfloat16))
        pooled = jnp.stack(pieces, axis=1)
        weight_shard = mix_weight[layer_idx]
        full_rows = lax.all_gather(weight_shard, "sp", axis=1, tiled=True)
        mixed_out = jnp.einsum(
            "rgc,gcn->rgn",
            pooled,
            lax.all_gather(full_rows, "tp", axis=2, tiled=True),
            preferred_element_type=jnp.float32,
        )
        residual = residual + mixed_out.reshape(row_count, feature_width) * branch_scale[layer_idx]
    return residual.astype(jnp.bfloat16)


def solution(mesh):
    return jax.shard_map(
        per_device,
        mesh=mesh,
        in_specs=(P(("grp", "sp", "tp"), None), P(), P(None, None, "sp", "tp"), P()),
        out_specs=P(("grp", "sp", "tp"), None),
        check_vma=False,
    )
```

profile of v0, /device:TPU:9, one launch (start us, length us, event | category | flops | bytes accessed | tf_op | source)
XLA Modules:
  0.0 248.3 jit_solution(16958773101239605890)
XLA Ops:
  6.5 0.0 all-gather.9.cloned.1.call-start
  6.5 2.2 fusion.69
  8.8 0.0 copy-start.1
  8.8 0.0 all-gather.9.cloned.1.call-update
  8.8 0.0 all-gather.13.cloned.1.call-start
  8.9 0.7 all-gather.13.cloned.1.call-update
  9.6 0.0 all-gather.11.cloned.1.call-start
  9.6 44.4 %all-gather.9.cloned.1.call-done = bf16[1,4,1024,256]{3,2,1,0:T(8,128)(2,1)} async-done(((bf16[1,4,256,256]{3,2,1,0:T(8,128)(2,1)}), bf16[1,4,1024,256]{3,2,1,0:T(8,128)(2,1)}) %all-gather.9.cloned.1.call-update) | async-done | bytes 2097168 | tf_op jit(solution)/shard_map/all_gather | solution.py:45
  54.0 0.0 all-gather.11.cloned.1.call-update
  54.0 0.0 all-gather.15.cloned.1.call-start
  54.0 0.0 copy-done.1
  54.0 0.7 fusion.4
  54.7 0.0 copy-start.3
  54.8 45.3 %all-gather.13.cloned.1.call-done = bf16[1,4,1024,256]{3,2,1,0:T(8,128)(2,1)} async-done(((bf16[1,4,256,256]{3,2,1,0:T(8,128)(2,1)}), bf16[1,4,1024,256]{3,2,1,0:T(8,128)(2,1)}) %all-gather.13.cloned.1.call-update) | async-done | bytes 2097168 | tf_op jit(solution)/shard_map/all_gather | solution.py:45
  100.0 0.0 all-gather.15.cloned.1.call-update
  100.0 0.0 copy-done.3
  100.1 0.0 copy-start.4
  100.1 1.0 fusion.6
  101.1 0.0 copy-start.2
  101.1 1.7 copy-done.2
  102.8 4.2 %collective-permute-start = (bf16[15,4096]{1,0:T(8,128)(2,1)S(1)}, bf16[15,4096]{1,0:T(8,128)(2,1)S(1)}, u32[]{:S(2)}, u32[]{:S(2)}) collective-permute-start(bf16[15,4096]{1,0:T(8,128)(2,1)S(1)} %slice.340), channel_id=1, source_target_pairs={{0,1},{1,2},{2,3},{3,4},{4,5},{5,6},{6,7},{7,8},{8,9},{9,10},{10,1... | collective-permute-start | bytes 368648 | tf_op jit(solution)/shard_map/ppermute | solution.py:17
  107.0 0.0 copy-done.4
  107.1 1.8 collective-permute-done
  108.9 3.2 %maximum_convert_fusion = f32[399,4096]{1,0:T(8,128)S(1)} fusion(bf16[384,4096]{1,0:T(8,128)(2,1)} %copy-done.2, bf16[15,4096]{1,0:T(8,128)(2,1)S(1)} %collective-permute-done), kind=kLoop, calls=%fused_computation.13 | loop fusion | flops 6537216 | bytes 9805824 | tf_op jit(solution)/shard_map/convert_element_type | solution.py:30
  112.2 3.3 %fusion.62 = bf16[384,1,1024]{2,0,1:T(8,128)(2,1)} fusion(f32[384]{0:T(512)S(1)} %fusion.63, f32[399,4096]{1,0:T(8,128)S(1)} %maximum_convert_fusion), kind=kLoop, calls=%fused_computation.114 | loop fusion | flops 7077888 | bytes 25953792 | tf_op jit(solution)/shard_map/stack | solution.py:43
  115.4 3.6 %fusion.56 = (bf16[384,1,1024]{2,0,1:T(8,128)(2,1)}, bf16[384,1,1024]{2,0,1:T(8,128)(2,1)}, bf16[384,1,1024]{2,0,1:T(8,128)(2,1)}) fusion(f32[384]{0:T(512)S(1)} %fusion.66, f32[399,4096]{1,0:T(8,128)S(1)} %maximum_convert_fusion, f32[384]{0:T(512)S(1)} %get-tuple-element.18, f32[384]{0:T(512)S(1)} %get-tuple-element.17), kind=kLoop, calls=%fused_computation.108 | loop fusion | flops 7864320 | bytes 24384000 | tf_op jit(solution)/shard_map/stack | solution.py:43
  119.0 43.0 %all-gather.11.cloned.1.call-done = bf16[1,4,1024,1024]{3,2,1,0:T(8,128)(2,1)} async-done(((bf16[1,4,1024,256]{3,2,1,0:T(8,128)(2,1)}), bf16[1,4,1024,1024]{3,2,1,0:T(8,128)(2,1)}) %all-gather.11.cloned.1.call-update) | async-done | bytes 8388624 | tf_op jit(solution)/shard_map/all_gather | solution.py:49
  162.0 7.8 %fusion.21 = f32[4,48,8,1024]{3,2,1,0:T(8,128)S(1)} fusion(bf16[1,4,1024,1024]{3,2,1,0:T(8,128)(2,1)} %all-gather.11.cloned.1.call-done, bf16[384,1,1024]{2,0,1:T(8,128)(2,1)} %fusion.62, bf16[384,1,1024]{2,0,1:T(8,128)(2,1)} %get-tuple-element.10, bf16[384,1,1024]{2,0,1:T(8,128)(2,1)} %get-tuple-element.9, bf16[384,1,1024]{2,0,1:T(8,128)(2,1)} %get-tuple-element.8), kind=kOutput, calls=%fused_computation.29 | convolution fusion | flops 3225944064 | bytes 17825792 | tf_op jit(solution)/shard_map/rgc,gcn->rgn/dot_general | solution.py:46
  169.8 0.6 copy.7
  170.4 0.0 copy-start
  170.4 1.2 multiply_reduce_fusion
  171.6 2.0 copy-done
  173.7 1.6 multiply_convert_fusion
  175.3 2.3 collective-permute-start.1
  177.6 4.6 %collective-permute-done.1 = bf16[15,4096]{1,0:T(8,128)(2,1)S(1)} collective-permute-done((bf16[15,4096]{1,0:T(8,128)(2,1)S(1)}, bf16[15,4096]{1,0:T(8,128)(2,1)S(1)}, u32[]{:S(2)}, u32[]{:S(2)}) %collective-permute-start.1) | collective-permute-done | bytes 122912 | tf_op jit(solution)/shard_map/ppermute | solution.py:17
  182.2 0.9 maximum_convert_fusion.1
  183.1 3.3 %fusion.61 = bf16[384,1,1024]{2,0,1:T(8,128)(2,1)} fusion(f32[384]{0:T(512)S(1)} %fusion.63, f32[399,4096]{1,0:T(8,128)S(1)} %maximum_convert_fusion.1), kind=kLoop, calls=%fused_computation.113 | loop fusion | flops 7077888 | bytes 25953792 | tf_op jit(solution)/shard_map/stack | solution.py:43
  186.4 3.5 %fusion.55 = (bf16[384,1,1024]{2,0,1:T(8,128)(2,1)}, bf16[384,1,1024]{2,0,1:T(8,128)(2,1)}, bf16[384,1,1024]{2,0,1:T(8,128)(2,1)}) fusion(f32[384]{0:T(512)S(1)} %fusion.66, f32[399,4096]{1,0:T(8,128)S(1)} %maximum_convert_fusion.1, f32[384]{0:T(512)S(1)} %get-tuple-element.18, f32[384]{0:T(512)S(1)} %get-tuple-element.17), kind=kLoop, calls=%fused_computation.107 | loop fusion | flops 7864320 | bytes 24384000 | tf_op jit(solution)/shard_map/stack | solution.py:43
  189.9 34.3 %all-gather.15.cloned.1.call-done = bf16[1,4,1024,1024]{3,2,1,0:T(8,128)(2,1)} async-done(((bf16[1,4,1024,256]{3,2,1,0:T(8,128)(2,1)}), bf16[1,4,1024,1024]{3,2,1,0:T(8,128)(2,1)}) %all-gather.15.cloned.1.call-update) | async-done | bytes 8388624 | tf_op jit(solution)/shard_map/all_gather | solution.py:49
  224.3 0.0 slice-start
  224.3 0.0 slice-start.1
  224.3 7.9 %fusion.26 = f32[4,48,8,1024]{3,2,1,0:T(8,128)S(1)} fusion(bf16[1,4,1024,1024]{3,2,1,0:T(8,128)(2,1)} %all-gather.15.cloned.1.call-done, bf16[384,1,1024]{2,0,1:T(8,128)(2,1)} %fusion.61, bf16[384,1,1024]{2,0,1:T(8,128)(2,1)} %get-tuple-element.7, bf16[384,1,1024]{2,0,1:T(8,128)(2,1)} %get-tuple-element.6, bf16[384,1,1024]{2,0,1:T(8,128)(2,1)} %get-tuple-element.5), kind=kOutput, calls=%fused_computation.30 | convolution fusion | flops 3225944064 | bytes 17825792 | tf_op jit(solution)/shard_map/rgc,gcn->rgn/dot_general | solution.py:46
  232.2 3.4 %copy.8 = f32[4,48,8,1024]{3,2,0,1:T(8,128)} copy(f32[4,48,8,1024]{3,2,1,0:T(8,128)S(1)} %fusion.26) | data formatting | bytes 12582912 | tf_op jit(solution)/shard_map/reshape | solution.py:52
  235.6 0.0 slice-done
  235.6 0.0 slice-done.1
  235.6 6.2 %add_convert_fusion = bf16[384,4096]{1,0:T(8,128)(2,1)} fusion(f32[384,4096]{1,0:T(8,128)} %bitcast.43, f32[4096]{0:T(1024)S(1)} %bitcast.47, f32[384,4096]{1,0:T(8,128)S(1)} %bitcast.42, f32[4096]{0:T(1024)S(1)} %bitcast.46, bf16[384,4096]{1,0:T(8,128)(2,1)S(1)} %copy-done.1), kind=kLoop, calls=%fused_computation.10 | loop fusion | flops 9437184 | bytes 18907136 | tf_op jit(solution)/shard_map/convert_element_type | solution.py:53
  (10 shorter events, 0.2 us)
Async XLA Ops:
  6.5 47.4 %all-gather.9.cloned.1.call-start = ((), (), s32[]{:S(2)}) async-start(), calls=%async_computation | async-start | bytes 2621440 | tf_op jit(solution)/shard_map/all_gather | solution.py:45
  8.8 45.3 %copy-start.1 = (bf16[384,4096]{1,0:T(8,128)(2,1)S(1)}, bf16[384,4096]{1,0:T(8,128)(2,1)}, u32[]{:S(2)}) copy-start(bf16[384,4096]{1,0:T(8,128)(2,1)} %param.4) | copy-start | bytes 9437188
  8.8 91.2 %all-gather.13.cloned.1.call-start = ((), (), s32[]{:S(2)}) async-start(), calls=%async_computation.2 | async-start | bytes 2621440 | tf_op jit(solution)/shard_map/all_gather | solution.py:45
  9.6 152.5 %all-gather.11.cloned.1.call-start = ((), (), s32[]{:S(2)}) async-start(), calls=%async_computation.1 | async-start | bytes 10485760 | tf_op jit(solution)/shard_map/all_gather | solution.py:49
  54.0 170.3 %all-gather.15.cloned.1.call-start = ((), (), s32[]{:S(2)}) async-start(), calls=%async_computation.3 | async-start | bytes 10485760 | tf_op jit(solution)/shard_map/all_gather | solution.py:49
  54.7 45.3 %copy-start.3 = (f32[2,4096]{1,0:T(2,128)S(1)}, f32[2,4096]{1,0:T(2,128)}, u32[]{:S(2)}) copy-start(f32[2,4096]{1,0:T(2,128)} %param.5) | copy-start | bytes 98308
  100.1 6.9 %copy-start.4 = (f32[2,4096]{1,0:T(2,128)S(1)}, f32[2,4096]{1,0:T(2,128)}, u32[]{:S(2)}) copy-start(f32[2,4096]{1,0:T(2,128)} %param.7) | copy-start | bytes 98308
  101.1 1.7 copy-start.2
  102.8 6.1 %collective-permute-start = (bf16[15,4096]{1,0:T(8,128)(2,1)S(1)}, bf16[15,4096]{1,0:T(8,128)(2,1)S(1)}, u32[]{:S(2)}, u32[]{:S(2)}) collective-permute-start(bf16[15,4096]{1,0:T(8,128)(2,1)S(1)} %slice.340), channel_id=1, source_target_pairs={{0,1},{1,2},{2,3},{3,4},{4,5},{5,6},{6,7},{7,8},{8,9},{9,10},{10,1... | collective-permute-start | bytes 368648 | tf_op jit(solution)/shard_map/ppermute | solution.py:17
  170.4 3.3 %copy-start = (f32[4,48,8,1024]{3,2,0,1:T(8,128)}, f32[4,48,8,1024]{3,2,0,1:T(8,128)S(1)}, u32[]{:S(2)}) copy-start(f32[4,48,8,1024]{3,2,0,1:T(8,128)S(1)} %copy.7) | copy-start | bytes 18874372
  175.3 6.9 %collective-permute-start.1 = (bf16[15,4096]{1,0:T(8,128)(2,1)S(1)}, bf16[15,4096]{1,0:T(8,128)(2,1)S(1)}, u32[]{:S(2)}, u32[]{:S(2)}) collective-permute-start(bf16[15,4096]{1,0:T(8,128)(2,1)S(1)} %slice.371), channel_id=1, source_target_pairs={{0,1},{1,2},{2,3},{3,4},{4,5},{5,6},{6,7},{7,8},{8,9},{9,10},{10,1... | collective-permute-start | bytes 368648 | tf_op jit(solution)/shard_map/ppermute | solution.py:17
  224.3 11.3 %slice-start = ((s8[6291456]{0:T(1024)(128)(4,1)}), s8[4194304]{0:T(1024)(128)(4,1)S(1)}, s32[]{:S(2)}) async-start(s8[6291456]{0:T(1024)(128)(4,1)} %bitcast.40), calls=%async_computation.4 | async-start | bytes 8388608
  224.3 11.3 %slice-start.1 = ((s8[6291456]{0:T(1024)(128)(4,1)}), s8[2097152]{0:T(1024)(128)(4,1)S(1)}, s32[]{:S(2)}) async-start(s8[6291456]{0:T(1024)(128)(4,1)} %bitcast.40), calls=%async_computation.5 | async-start | bytes 4194304
Sparse Core Ops, SparseCore 0:
  8.9 44.9 all-gather.8
  55.5 44.4 all-gather.12
  101.6 60.4 all-gather.10
  163.4 60.7 all-gather.14
where the time goes:
time: 249 us; the launch traced here: 248 us
  waiting for transfers between devices  174 us (70%)
  other arithmetic  28.5 us (11%)
  matrix products  15.6 us (6%)
  between operations  13.3 us (5%)
  local copies, waits for them, and re-layouts  10.1 us (4%)
  starting transfers between devices  6.56 us (3%)
    all_gather x2, waiting for transfers between devices, per_device(): full_rows = lax.all_gather(weight_shard, 'sp', axis=1, tiled=True)  89.6 us
    all_gather x2, waiting for transfers between devices, per_device(): lax.all_gather(full_rows, 'tp', axis=2, tiled=True)  77.3 us
    dot_general x2, matrix products, per_device(): jnp.einsum('rgc,gcn->rgn', pooled, lax.all_gather(full_rows, 'tp', axis=2...  15.6 us
    another operation x4, other arithmetic, per_device(): pooled = jnp.stack(pieces, axis=1)  13.6 us
    ppermute x2, waiting for transfers between devices, from_behind(): return lax.ppermute(block, axis, route)  6.48 us
    ppermute x2, starting transfers between devices, from_behind(): return lax.ppermute(block, axis, route)  6.44 us
    convert_element_type x1, other arithmetic, per_device(): return residual.astype(jnp.bfloat16)  6.2 us
  transfers between devices with their start and end apart: 6, of which 6 were waited for; matrix products, arithmetic and copies ran while one was open for 12% of the time, Pallas kernels for 0%

commit v1 on v0

--- a/solution.py
+++ b/solution.py
@@ -46,7 +46,7 @@
         mixed_out = jnp.einsum(
             "rgc,gcn->rgn",
             pooled,
-            lax.all_gather(full_rows, "tp", axis=2, tiled=True),
+            jnp.concatenate(lax.all_gather(full_rows, "tp"), axis=2),
             preferred_element_type=jnp.float32,
         )
         residual = residual + mixed_out.reshape(row_count, feature_width) * branch_scale[layer_idx]

time: 249 us -> 256 us (1.028)
  local copies, waits for them, and re-layouts: 10.1 us -> 27.1 us
  matrix products: 15.6 us -> 11.1 us
  waiting for transfers between devices: 174 us -> 171 us
    reshape x0 -> x2, local copies, waits for them, and re-layouts: none -> 15.9 us  [per_device(): jnp.concatenate(lax.all_gather(full_rows, 'tp'), axis=2)]
    ppermute x2, waiting for transfers between devices: 6.48 us -> 1.84 us  [from_behind(): return lax.ppermute(block, axis, route)]
    dot_general x2, matrix products: 15.6 us -> 11.1 us  [per_device(): jnp.einsum('rgc,gcn->rgn', pooled, jnp.concatenate(lax.all_gather(full_ro...]
  transfers between devices with their start and end apart: 6 -> 6, of which waited for: 6 -> 5; matrix products, arithmetic and copies ran while one was open for 12% -> 15% of each run, Pallas kernels for 0% -> 0%
where the time goes in v1:
time: 256 us
  waiting for transfers between devices  171 us (67%)
  local copies, waits for them, and re-layouts  27.1 us (11%)
  other arithmetic  27.1 us (11%)
  between operations  13.4 us (5%)
  matrix products  11.1 us (4%)
  starting transfers between devices  6.73 us (3%)
    all_gather x2, waiting for transfers between devices, per_device(): full_rows = lax.all_gather(weight_shard, 'sp', axis=1, tiled=True)  90.3 us
    all_gather x2, waiting for transfers between devices, per_device(): lax.all_gather(full_rows, 'tp')  77.7 us
    reshape x2, local copies, waits for them, and re-layouts, per_device(): jnp.concatenate(lax.all_gather(full_rows, 'tp'), axis=2)  15.9 us
    another operation x4, other arithmetic, per_device(): pooled = jnp.stack(pieces, axis=1)  12.1 us
    dot_general x2, matrix products, per_device(): jnp.einsum('rgc,gcn->rgn', pooled, jnp.concatenate(lax.all_gather(full_ro...  11.1 us
    ppermute x2, starting transfers between devices, from_behind(): return lax.ppermute(block, axis, route)  6.61 us
    convert_element_type x1, other arithmetic, per_device(): return residual.astype(jnp.bfloat16)  6.2 us
  transfers between devices with their start and end apart: 6, of which 5 were waited for; matrix products, arithmetic and copies ran while one was open for 15% of the time, Pallas kernels for 0%

profile of v1, /device:TPU:9, one launch (start us, length us, event | category | flops | bytes accessed | tf_op | source)
XLA Modules:
  0.0 256.0 jit_solution(15359959572065421662)
XLA Ops:
  6.5 0.0 all-gather.9.cloned.1.call-start
  6.5 2.3 fusion.63
  8.8 0.0 all-gather.9.cloned.1.call-update
  8.8 0.0 all-gather.13.cloned.1.call-start
  8.9 0.7 all-gather.13.cloned.1.call-update
  9.6 0.0 all-gather.11.cloned.1.call-start
  9.6 44.4 %all-gather.9.cloned.1.call-done = bf16[1,4,1024,256]{3,2,1,0:T(8,128)(2,1)} async-done(((bf16[1,4,256,256]{3,2,1,0:T(8,128)(2,1)}), bf16[1,4,1024,256]{3,2,1,0:T(8,128)(2,1)}) %all-gather.9.cloned.1.call-update) | async-done | bytes 2097168 | tf_op jit(solution)/shard_map/all_gather | solution.py:45
  54.0 0.0 copy-start.1
  54.0 0.0 all-gather.11.cloned.1.call-update
  54.0 0.0 all-gather.15.cloned.1.call-start
  54.0 46.0 %all-gather.13.cloned.1.call-done = bf16[1,4,1024,256]{3,2,1,0:T(8,128)(2,1)} async-done(((bf16[1,4,256,256]{3,2,1,0:T(8,128)(2,1)}), bf16[1,4,1024,256]{3,2,1,0:T(8,128)(2,1)}) %all-gather.13.cloned.1.call-update) | async-done | bytes 2097168 | tf_op jit(solution)/shard_map/all_gather | solution.py:45
  100.0 0.0 all-gather.15.cloned.1.call-update
  100.1 0.0 copy-done.1
  100.1 0.0 copy-start.9
  100.1 0.7 fusion
  100.8 0.0 copy-done.9
  100.9 0.0 copy-start.10
  100.9 1.0 fusion.2
  101.9 0.0 copy-start.2
  101.9 1.7 copy-done.2
  103.6 4.2 %collective-permute-start = (bf16[15,4096]{1,0:T(8,128)(2,1)S(1)}, bf16[15,4096]{1,0:T(8,128)(2,1)S(1)}, u32[]{:S(2)}, u32[]{:S(2)}) collective-permute-start(bf16[15,4096]{1,0:T(8,128)(2,1)S(1)} %slice.340), channel_id=1, source_target_pairs={{0,1},{1,2},{2,3},{3,4},{4,5},{5,6},{6,7},{7,8},{8,9},{9,10},{10,1... | collective-permute-start | bytes 368648 | tf_op jit(solution)/shard_map/ppermute | solution.py:17
  107.8 0.0 copy-done.10
  107.8 1.8 collective-permute-done
  109.7 3.3 %maximum_convert_fusion = f32[399,4096]{1,0:T(8,128)S(1)} fusion(bf16[384,4096]{1,0:T(8,128)(2,1)} %copy-done.2, bf16[15,4096]{1,0:T(8,128)(2,1)S(1)} %collective-permute-done), kind=kLoop, calls=%fused_computation.9 | loop fusion | flops 6537216 | bytes 9805824 | tf_op jit(solution)/shard_map/convert_element_type | solution.py:30
  113.0 3.3 %fusion.56 = bf16[384,1,1024]{2,0,1:T(8,128)(2,1)} fusion(f32[384]{0:T(512)S(1)} %fusion.57, f32[399,4096]{1,0:T(8,128)S(1)} %maximum_convert_fusion), kind=kLoop, calls=%fused_computation.112 | loop fusion | flops 7077888 | bytes 25953792 | tf_op jit(solution)/shard_map/stack | solution.py:43
  116.3 3.6 %fusion.50 = (bf16[384,1,1024]{2,0,1:T(8,128)(2,1)}, bf16[384,1,1024]{2,0,1:T(8,128)(2,1)}, bf16[384,1,1024]{2,0,1:T(8,128)(2,1)}) fusion(f32[384]{0:T(512)S(1)} %fusion.60, f32[399,4096]{1,0:T(8,128)S(1)} %maximum_convert_fusion, f32[384]{0:T(512)S(1)} %get-tuple-element.18, f32[384]{0:T(512)S(1)} %get-tuple-element.17), kind=kLoop, calls=%fused_computation.106 | loop fusion | flops 7864320 | bytes 24384000 | tf_op jit(solution)/shard_map/stack | solution.py:43
  119.8 41.1 %all-gather.11.cloned.1.call-done = bf16[4,4,1024,256]{3,2,1,0:T(8,128)(2,1)} async-done(((bf16[1,4,1024,256]{3,2,1,0:T(8,128)(2,1)}), bf16[4,4,1024,256]{3,2,1,0:T(8,128)(2,1)}) %all-gather.11.cloned.1.call-update) | async-done | bytes 8388624 | tf_op jit(solution)/shard_map/all_gather | solution.py:49
  160.9 0.0 copy-start.5
  160.9 0.0 copy-start.6
  160.9 0.0 copy-start.7
  160.9 0.0 copy-start.8
  160.9 8.0 %copy.13 = bf16[4,4,128,8,256]{4,3,0,2,1:T(8,128)(2,1)} copy(bf16[4,4,128,8,256]{4,3,2,1,0:T(8,128)(2,1)} %bitcast.43) | data formatting | bytes 16777216 | tf_op jit(solution)/shard_map/reshape | solution.py:49
  168.9 0.0 copy-done.5
  168.9 0.0 copy-done.6
  168.9 0.0 copy-done.7
  168.9 0.0 copy-done.8
  168.9 7.6 %fusion.22 = f32[4,48,8,1024]{3,2,1,0:T(8,128)S(1)} fusion(bf16[4,1024,1024]{2,1,0:T(8,128)(2,1)} %bitcast.47, bf16[384,1,1024]{2,0,1:T(8,128)(2,1)S(1)} %copy-done.5, bf16[384,1,1024]{2,0,1:T(8,128)(2,1)S(1)} %copy-done.8, bf16[384,1,1024]{2,0,1:T(8,128)(2,1)S(1)} %copy-done.7, bf16[384,1,1024]{2,0,1:T(8,128)(2,1)S(1)} %copy-done.6), kind=kOutput, calls=%fused_computation.28 | convolution fusion | flops 3225944064 | bytes 17825792 | tf_op jit(solution)/shard_map/rgc,gcn->rgn/dot_general | solution.py:46
  176.5 0.6 copy.14
  177.1 0.0 copy-start
  177.1 1.2 multiply_reduce_fusion
  178.3 1.4 copy-done
  179.7 1.6 multiply_convert_fusion
  181.3 0.0 copy-start.3
  181.3 1.7 copy-done.3
  183.0 2.4 collective-permute-start.1
  185.4 36.6 %all-gather.15.cloned.1.call-done = bf16[4,4,1024,256]{3,2,1,0:T(8,128)(2,1)} async-done(((bf16[1,4,1024,256]{3,2,1,0:T(8,128)(2,1)}), bf16[4,4,1024,256]{3,2,1,0:T(8,128)(2,1)}) %all-gather.15.cloned.1.call-update) | async-done | bytes 8388624 | tf_op jit(solution)/shard_map/all_gather | solution.py:49
  222.0 0.0 copy-start.4
  222.0 7.9 %copy.15 = bf16[4,4,128,8,256]{4,3,0,2,1:T(8,128)(2,1)} copy(bf16[4,4,128,8,256]{4,3,2,1,0:T(8,128)(2,1)} %bitcast.42) | data formatting | bytes 16777216 | tf_op jit(solution)/shard_map/reshape | solution.py:49
  230.0 0.0 collective-permute-done.1
  230.0 0.0 copy-done.4
  230.0 0.9 maximum_convert_fusion.1
  230.9 0.0 slice-start.2
  230.9 2.8 %fusion.49 = (bf16[384,1,1024]{2,0,1:T(8,128)(2,1)S(1)}, bf16[384,1,1024]{2,0,1:T(8,128)(2,1)S(1)}, bf16[384,1,1024]{2,0,1:T(8,128)(2,1)S(1)}) fusion(f32[384]{0:T(512)S(1)} %fusion.60, f32[399,4096]{1,0:T(8,128)S(1)} %maximum_convert_fusion.1, f32[384]{0:T(512)S(1)} %get-tuple-element.18, f32[384]{0:T(512)S(1)} %get-tuple-element.17), kind=kLoop, calls=%fused_computation.105 | loop fusion | flops 7864320 | bytes 24384000 | tf_op jit(solution)/shard_map/stack | solution.py:43
  233.7 0.0 slice-start.3
  233.7 2.5 fusion.55
  236.3 0.0 slice-start
  236.3 0.0 slice-done.2
  236.3 0.0 slice-done.3
  236.3 0.0 slice-start.1
  236.3 3.5 %fusion.19 = f32[4,48,8,1024]{3,2,1,0:T(8,128)S(1)} fusion(bf16[4,1024,1024]{2,1,0:T(8,128)(2,1)S(1)} %bitcast.46, bf16[384,1,1024]{2,0,1:T(8,128)(2,1)S(1)} %fusion.55, bf16[384,1,1024]{2,0,1:T(8,128)(2,1)S(1)} %get-tuple-element.7, bf16[384,1,1024]{2,0,1:T(8,128)(2,1)S(1)} %get-tuple-element.6, bf16[384,1,1024]{2,0,1:T(8,128)(2,1)S(1)} %get-tuple-element.5), kind=kOutput, calls=%fused_computation.27 | convolution fusion | flops 3225944064 | bytes 17825792 | tf_op jit(solution)/shard_map/rgc,gcn->rgn/dot_general | solution.py:46
  239.8 3.4 %copy.16 = f32[4,48,8,1024]{3,2,0,1:T(8,128)} copy(f32[4,48,8,1024]{3,2,1,0:T(8,128)S(1)} %fusion.19) | data formatting | bytes 12582912 | tf_op jit(solution)/shard_map/reshape | solution.py:52
  243.2 0.0 slice-done
  243.2 0.0 slice-done.1
  243.2 6.2 %add_convert_fusion = bf16[384,4096]{1,0:T(8,128)(2,1)} fusion(f32[384,4096]{1,0:T(8,128)} %bitcast.41, f32[4096]{0:T(1024)S(1)} %bitcast.51, f32[384,4096]{1,0:T(8,128)S(1)} %bitcast.40, f32[4096]{0:T(1024)S(1)} %bitcast.50, bf16[384,4096]{1,0:T(8,128)(2,1)S(1)} %copy-done.1), kind=kLoop, calls=%fused_computation.6 | loop fusion | flops 9437184 | bytes 18907136 | tf_op jit(solution)/shard_map/convert_element_type | solution.py:53
  (11 shorter events, 0.2 us)
Async XLA Ops:
  6.5 47.4 %all-gather.9.cloned.1.call-start = ((), (), s32[]{:S(2)}) async-start(), calls=%async_computation | async-start | bytes 2621440 | tf_op jit(solution)/shard_map/all_gather | solution.py:45
  8.8 91.2 %all-gather.13.cloned.1.call-start = ((), (), s32[]{:S(2)}) async-start(), calls=%async_computation.2 | async-start | bytes 2621440 | tf_op jit(solution)/shard_map/all_gather | solution.py:45
  9.6 151.4 %all-gather.11.cloned.1.call-start = ((), (), s32[]{:S(2)}) async-start(), calls=%async_computation.1 | async-start | bytes 10485760 | tf_op jit(solution)/shard_map/all_gather | solution.py:49
  54.0 46.1 %copy-start.1 = (bf16[384,4096]{1,0:T(8,128)(2,1)S(1)}, bf16[384,4096]{1,0:T(8,128)(2,1)}, u32[]{:S(2)}) copy-start(bf16[384,4096]{1,0:T(8,128)(2,1)} %param.4) | copy-start | bytes 9437188
  54.0 168.0 %all-gather.15.cloned.1.call-start = ((), (), s32[]{:S(2)}) async-start(), calls=%async_computation.3 | async-start | bytes 10485760 | tf_op jit(solution)/shard_map/all_gather | solution.py:49
  100.1 0.8 copy-start.9
  100.9 6.9 %copy-start.10 = (f32[2,4096]{1,0:T(2,128)S(1)}, f32[2,4096]{1,0:T(2,128)}, u32[]{:S(2)}) copy-start(f32[2,4096]{1,0:T(2,128)} %param.7) | copy-start | bytes 98308
  101.9 1.7 copy-start.2
  103.6 6.1 %collective-permute-start = (bf16[15,4096]{1,0:T(8,128)(2,1)S(1)}, bf16[15,4096]{1,0:T(8,128)(2,1)S(1)}, u32[]{:S(2)}, u32[]{:S(2)}) collective-permute-start(bf16[15,4096]{1,0:T(8,128)(2,1)S(1)} %slice.340), channel_id=1, source_target_pairs={{0,1},{1,2},{2,3},{3,4},{4,5},{5,6},{6,7},{7,8},{8,9},{9,10},{10,1... | collective-permute-start | bytes 368648 | tf_op jit(solution)/shard_map/ppermute | solution.py:17
  160.9 8.0 %copy-start.5 = (bf16[384,1,1024]{2,0,1:T(8,128)(2,1)S(1)}, bf16[384,1,1024]{2,0,1:T(8,128)(2,1)}, u32[]{:S(2)}) copy-start(bf16[384,1,1024]{2,0,1:T(8,128)(2,1)} %fusion.56) | copy-start | bytes 2359300
  160.9 8.0 %copy-start.6 = (bf16[384,1,1024]{2,0,1:T(8,128)(2,1)S(1)}, bf16[384,1,1024]{2,0,1:T(8,128)(2,1)}, u32[]{:S(2)}) copy-start(bf16[384,1,1024]{2,0,1:T(8,128)(2,1)} %get-tuple-element.8) | copy-start | bytes 2359300
  160.9 8.0 %copy-start.7 = (bf16[384,1,1024]{2,0,1:T(8,128)(2,1)S(1)}, bf16[384,1,1024]{2,0,1:T(8,128)(2,1)}, u32[]{:S(2)}) copy-start(bf16[384,1,1024]{2,0,1:T(8,128)(2,1)} %get-tuple-element.9) | copy-start | bytes 2359300
  160.9 8.0 %copy-start.8 = (bf16[384,1,1024]{2,0,1:T(8,128)(2,1)S(1)}, bf16[384,1,1024]{2,0,1:T(8,128)(2,1)}, u32[]{:S(2)}) copy-start(bf16[384,1,1024]{2,0,1:T(8,128)(2,1)} %get-tuple-element.10) | copy-start | bytes 2359300
  177.1 2.6 %copy-start = (f32[4,48,8,1024]{3,2,0,1:T(8,128)}, f32[4,48,8,1024]{3,2,0,1:T(8,128)S(1)}, u32[]{:S(2)}) copy-start(f32[4,48,8,1024]{3,2,0,1:T(8,128)S(1)} %copy.14) | copy-start | bytes 18874372
  181.3 1.7 copy-start.3
  183.0 47.0 %collective-permute-start.1 = (bf16[15,4096]{1,0:T(8,128)(2,1)S(1)}, bf16[15,4096]{1,0:T(8,128)(2,1)S(1)}, u32[]{:S(2)}, u32[]{:S(2)}) collective-permute-start(bf16[15,4096]{1,0:T(8,128)(2,1)S(1)} %slice.371), channel_id=1, source_target_pairs={{0,1},{1,2},{2,3},{3,4},{4,5},{5,6},{6,7},{7,8},{8,9},{9,10},{10,1... | collective-permute-start | bytes 368648 | tf_op jit(solution)/shard_map/ppermute | solution.py:17
  222.0 7.9 %copy-start.4 = (bf16[384,4096]{1,0:T(8,128)(2,1)S(1)}, bf16[384,4096]{1,0:T(8,128)(2,1)}, u32[]{:S(2)}) copy-start(bf16[384,4096]{1,0:T(8,128)(2,1)} %copy-done.3) | copy-start | bytes 9437188
  230.9 5.4 %slice-start.2 = ((s8[8388608]{0:T(1024)(128)(4,1)}), s8[4194304]{0:T(1024)(128)(4,1)S(1)}, s32[]{:S(2)}) async-start(s8[8388608]{0:T(1024)(128)(4,1)} %bitcast.44), calls=%async_computation.6 | async-start | bytes 8388608
  233.7 2.6 %slice-start.3 = ((s8[8388608]{0:T(1024)(128)(4,1)}), s8[4194304]{0:T(1024)(128)(4,1)S(1)}, s32[]{:S(2)}) async-start(s8[8388608]{0:T(1024)(128)(4,1)} %bitcast.44), calls=%async_computation.7 | async-start | bytes 8388608
  236.3 7.0 %slice-start = ((s8[6291456]{0:T(1024)(128)(4,1)}), s8[4194304]{0:T(1024)(128)(4,1)S(1)}, s32[]{:S(2)}) async-start(s8[6291456]{0:T(1024)(128)(4,1)} %bitcast.38), calls=%async_computation.4 | async-start | bytes 8388608
  236.3 6.9 %slice-start.1 = ((s8[6291456]{0:T(1024)(128)(4,1)}), s8[2097152]{0:T(1024)(128)(4,1)S(1)}, s32[]{:S(2)}) async-start(s8[6291456]{0:T(1024)(128)(4,1)} %bitcast.38), calls=%async_computation.5 | async-start | bytes 4194304
Sparse Core Ops, SparseCore 0:
  8.9 44.9 all-gather.8
  55.5 44.4 all-gather.12
  101.6 59.2 all-gather.10
  162.3 59.6 all-gather.14
